TPU v7x, 32 devices: a whole 2x2x4 slice. The times are simulated.
32 devices in a mesh: grp: 2 (over y), sp: 16 (over z, x, core), tp: 1.
Axes of the slice: x: 2, y: 2, z: 4, core: 2. Of those that a mesh axis runs over, the one named last changes fastest.
Arguments:
- resid: bfloat16 [8192, 2048], P(('grp', 'sp', 'tp')), parts along dimension 0, may hold values from -6 to 6
- gate_b: bfloat16 [8192, 2048], P(('grp', 'sp'), 'tp'), parts along dimension 0, may hold values from -6 to 6
- gate_c: bfloat16 [8192, 2048], P(('grp', 'sp'), 'tp'), parts along dimension 0, may hold values from -6 to 6
- value: bfloat16 [8192, 2048], P(('grp', 'sp'), 'tp'), parts along dimension 0, may hold values from -6 to 6
- taps: bfloat16 [3, 2048], P(None, 'tp'), may hold values from -3.5 to 3.5
- doc_ids: int32 [8192], P(('grp', 'sp')), parts along dimension 0, may hold values from 0 to 3, never falling along the last dimension, each value on 1 to 2048 neighbouring positions
- out_weight: bfloat16 [2048, 2048], P('tp'), may hold values from -0.125 to 0.125
- norm_gains: float32 [3, 2048], replicated, may hold values from 0.1 to 1.9
- routes: int32 [8192, 2], P(('grp', 'sp')), parts along dimension 0, may hold values from 0 to 15, all different within a row; in each aligned block of 256 rows (0 to 255, 256 to 511, ...) at most 48 rows name the same one
- route_weights: float32 [8192, 2], P(('grp', 'sp')), parts along dimension 0, may hold values from 0.2 to 1
- w_gate: bfloat16 [16, 2048, 4096], P('sp', None, 'tp'), may hold values from -0.125 to 0.125
- w_up: bfloat16 [16, 2048, 4096], P('sp', None, 'tp'), may hold values from -0.125 to 0.125
- w_down: bfloat16 [16, 4096, 2048], P('sp', 'tp'), may hold values from -0.09375 to 0.09375
Outputs:
- layer_out: bfloat16 [8192, 2048], P(('grp', 'sp', 'tp')), parts along dimension 0
There are 2 independent parts, one for each index of `grp`. A program takes and returns all parts, laid end to end along the dimension named above; an argument that names none is the same for every part. Nothing has to cross between parts.
Inputs may be any that keep to these rules, and one draw needn't show every extreme that they name: `doc_ids`: never falling along the sequence; each document spans 1 to 2048 positions. `routes`: each row names 2 different experts. In each aligned block of 256 rows no expert is named more than 48 times, and in every draw some block names some expert exactly 48 times.
All inputs are finite; a program needn't handle non-finite values.
Results may differ from a plain program's by a relative error of at most 0.02.
Values may be sent and summed in bfloat16 or wider, within the bound.
A program may use at most 128 MiB of HBM per device.

v0:
```python
import functools

import jax
import jax.numpy as jnp
import numpy as np
from jax import lax
from jax.experimental import pallas as pl
from jax.experimental.pallas import tpu as pltpu
from jax.sharding import PartitionSpec as P

TAPS = 3
TOP = 2


norm_eps = 1e-06


def passed_along(block, axis, distance):
    devices = range(lax.axis_size(axis))
    route = [(i - distance, i) for i in devices if i - distance in devices]
    return lax.ppermute(block, axis, route)


def rms_scale(values, gain_row):
    mean_sq = jnp.mean(values * values, axis=-1, keepdims=True)
    return values * lax.rsqrt(mean_sq + norm_eps) * gain_row


def slot_table(block_routes, experts, capacity):
    block_count = block_routes.shape[0]
    block_len = block_routes.shape[1]
    flat_routes = block_routes.reshape(block_count, block_len * TOP)
    onehot = (
        flat_routes[:, :, None] == jnp.arange(experts, dtype=jnp.int32)[None, None, :]
    ).astype(jnp.int32)
    before = jnp.cumsum(onehot, axis=1) - onehot
    slot_rank = jnp.sum(before * onehot, axis=2)
    slot_hit = onehot[:, :, :, None] * (
        slot_rank[:, :, None, None] == jnp.arange(capacity, dtype=jnp.int32)[None, None, None, :]
    ).astype(jnp.int32)
    owner_row = jnp.arange(block_len * TOP, dtype=jnp.int32) // TOP
    slot_tok = jnp.sum(slot_hit * owner_row[None, :, None, None], axis=1)
    filled = jnp.sum(slot_hit, axis=1)
    return (slot_rank.reshape(block_count, block_len, TOP), slot_tok, filled)


def pick_rows(normed_rows, slot_tok, filled):
    picked_rows = normed_rows[slot_tok]
    return jnp.where(filled[:, :, None] > 0, picked_rows, jnp.zeros_like(picked_rows))


def expert_hidden(picked_rows, w_gate, w_up):
    gate_proj = jnp.dot(picked_rows, w_gate[0], preferred_element_type=jnp.float32)
    up_proj = jnp.dot(picked_rows, w_up[0], preferred_element_type=jnp.float32)
    return (jax.nn.silu(gate_proj) * up_proj).astype(jnp.bfloat16)


def per_device_split(
    resid,
    gate_b,
    gate_c,
    value,
    taps,
    doc_ids,
    out_weight,
    norm_gains,
    routes,
    route_weights,
    w_gate,
    w_up,
    w_down,
):
    tok_dev = gate_b.shape[0]
    rows_blk = resid.shape[0]
    model_width = resid.shape[1]
    experts = lax.axis_size("sp")
    capacity = max(2, 3 * TOP * rows_blk // (2 * experts))
    tap_reach = TAPS - 1
    product = gate_c.astype(jnp.float32) * value.astype(jnp.float32)
    id_values = doc_ids.astype(jnp.float32)
    prev_rows, prev_ids = passed_along(
        (product[tok_dev - tap_reach :], id_values[tok_dev - tap_reach :]), "sp", 1
    )
    ext_rows = jnp.concatenate([prev_rows, product], axis=0)
    ext_ids = jnp.concatenate([prev_ids, id_values], axis=0)
    tap_weights = taps.astype(jnp.float32)
    convolved = tap_weights[0] * product
    for distance in range(1, TAPS):
        earlier = ext_rows[tap_reach - distance : tap_reach - distance + tok_dev]
        same_doc = ext_ids[tap_reach - distance : tap_reach - distance + tok_dev] == id_values
        convolved = convolved + jnp.where(same_doc[:, None], tap_weights[distance] * earlier, 0.0)
    mixed_rows = (gate_b.astype(jnp.float32) * convolved).astype(jnp.bfloat16)
    block_rows = mixed_rows
    projected = lax.psum_scatter(
        jnp.dot(block_rows, out_weight, preferred_element_type=jnp.float32).astype(jnp.bfloat16),
        "tp",
        scatter_dimension=0,
        tiled=True,
    ).astype(jnp.float32)
    stream = resid.astype(jnp.float32) + rms_scale(projected, norm_gains[0])
    normed = rms_scale(stream, norm_gains[1]).astype(jnp.bfloat16)
    lane_index = lax.axis_index("tp")
    offset = lane_index * rows_blk
    my_routes = lax.dynamic_slice_in_dim(routes, offset, rows_blk, 0)
    my_weights = lax.dynamic_slice_in_dim(route_weights, offset, rows_blk, 0)
    own_rank, own_tok, own_filled = slot_table(my_routes[None], experts, capacity)
    slot_rank = own_rank[0]
    outgoing = pick_rows(normed, own_tok[0], own_filled[0])
    arrived = lax.all_to_all(outgoing, "sp", split_axis=0, concat_axis=0, tiled=True)
    hidden = expert_hidden(
        lax.all_gather(arrived[None], "tp", axis=0, tiled=True).reshape(-1, model_width),
        w_gate,
        w_up,
    )
    block_rows = hidden
    summed = lax.psum_scatter(
        jnp.dot(block_rows, w_down[0], preferred_element_type=jnp.float32).astype(jnp.bfloat16),
        "tp",
        scatter_dimension=0,
        tiled=True,
    )
    results = summed.reshape(experts, capacity, model_width)
    returned = lax.all_to_all(results, "sp", split_axis=0, concat_axis=0, tiled=True)
    picked = returned[my_routes, slot_rank]
    shares = my_weights / jnp.sum(my_weights, axis=1, keepdims=True)
    combined = jnp.sum(shares[:, :, None] * picked.astype(jnp.float32), axis=1)
    return (stream + rms_scale(combined, norm_gains[2])).astype(jnp.bfloat16)


MESH = pl.DeviceIdType.MESH


def flipped(me, distance, n):
    out, bit = 0, 1
    while bit < n:
        digit = (me // bit) % 2
        if distance & bit:
            digit = 1 - digit
        out = out + digit * bit
        bit *= 2
    return out


def expert_kernel(
    n, cap, tile, down_tile, chunk,
    rows_hbm, normed_hbm, meta_hbm, gate_hbm, up_hbm, down_hbm,
    weights_v, spread_v, spread_t, wanted_row, wanted_col, stream_hbm, gain_v, out_v,
    gate_v, up_v, down_v, arrived, hidden, near_back, far_sum, tokens, picked, relay_back,
    meta_v, chosen_t, relay_weights, stream_v, total,
    gate_sem, up_sem, down_sem, tok_send, tok_recv, meta_send, meta_recv,
    near_send, near_recv, pick_send, pick_recv, back_send, back_recv,
    far_send, far_recv, sum_send, sum_recv, own_sem,
):
    me = lax.axis_index("sp")
    quarter, half = n // 4, n // 2
    plane, spot = me // quarter, me % quarter
    side = plane // 2
    relaying = (plane + side) % 2
    units = gate_v.shape[1]
    width = normed_hbm.shape[1]
    depth = down_v.shape[0]
    chunks = width // chunk
    down_tiles = width // down_tile
    far_relay = (2 - side) * quarter + spot
    my_turn = 1 - relaying

    def source_of(s):
        return ((2 - side) + s * (1 - 2 * side)) * quarter + spot

    def columns(t, size):
        return pl.ds(pl.multiple_of(t * size, size), size)

    def load(src, dst, sem, t, size):
        cols = columns(t, size)
        return pltpu.make_async_copy(src.at[0, :, cols], dst.at[:, cols], sem.at[t])

    def load_down(step):
        return pltpu.make_async_copy(
            down_hbm.at[0, :, columns(step % down_tiles, down_tile)],
            down_v.at[step % depth],
            down_sem.at[step % depth],
        )

    def remote(src, dst, sent, got, device):
        return pltpu.make_async_remote_copy(
            src_ref=src, dst_ref=dst, send_sem=sent, recv_sem=got,
            device_id={"sp": device}, device_id_type=MESH,
        )

    def settle(ref, sem):
        pltpu.make_async_copy(ref, ref, sem).wait()

    def block(i, count=1):
        return pl.ds(i * cap, count * cap)

    barrier = pltpu.get_barrier_semaphore()

    def greet(device):
        pl.semaphore_signal(barrier, inc=1, device_id={"sp": device}, device_id_type=MESH)

    for d in range(1, half):
        greet(flipped(me, d, n))
    greet(far_relay)

    @pl.when(relaying == 1)
    def _():
        greet(source_of(0))
        greet(source_of(1))

    own_rows = pltpu.make_async_copy(rows_hbm.at[block(0)], arrived.at[block(0)], own_sem.at[0])
    own_rows.start()
    for t in range(units // tile):
        load(gate_hbm, gate_v, gate_sem, t, tile).start()
        load(up_hbm, up_v, up_sem, t, tile).start()
    for t in range(depth):
        load_down(t).start()
    stream_in = pltpu.make_async_copy(stream_hbm, stream_v, own_sem.at[1])
    stream_in.start()
    pl.semaphore_wait(barrier, half + 2 * relaying)

    def send_tokens():
        remote(
            meta_hbm, meta_v.at[my_turn], meta_send.at[0], meta_recv.at[my_turn], far_relay
        ).start()
        for c in range(chunks):
            cols = pl.ds(c * chunk, chunk)
            remote(
                normed_hbm.at[:, cols], tokens.at[my_turn, :, cols],
                tok_send.at[0], tok_recv.at[my_turn * chunks + c], far_relay,
            ).start()

    def send_near(distances):
        for d in distances:
            remote(
                rows_hbm.at[block(d)], arrived.at[block(d)],
                near_send.at[0], near_recv.at[d // quarter], flipped(me, d, n),
            ).start()

    @pl.when(relaying == 1)
    def _():
        send_tokens()

    send_near(list(range(1, quarter)) + list(range(quarter, half)))

    @pl.when(relaying == 0)
    def _():
        send_tokens()

    def pick(s, c):
        cols = columns(c, chunk)
        settle(tokens.at[s, :, cols], tok_recv.at[s * chunks + c])
        if s > 0:
            settle(picked.at[block(1, half - 1), cols], pick_send.at[c])
        rows = jnp.dot(
            chosen_t[...], tokens[s, :, cols], preferred_element_type=jnp.float32
        ).astype(jnp.bfloat16)
        arrived[block(half + s * quarter), cols] = rows[:cap]
        picked[pl.ds(cap, (half - 1) * cap), cols] = rows[cap:]
        for d in list(range(quarter, half)) + list(range(1, quarter)):
            remote(
                picked.at[block(d), cols],
                arrived.at[block(half + s * quarter + d % quarter), cols],
                pick_send.at[c], pick_recv.at[s * chunks + c], flipped(me, d, n),
            ).start()

    def read_meta(s):
        settle(meta_v.at[s], meta_recv.at[s])
        places = meta_v[s, :half].astype(jnp.bfloat16)
        shares = meta_v[s, half:].astype(jnp.bfloat16)
        chosen_t[...] = (
            jnp.dot(spread_t[...], places, preferred_element_type=jnp.float32) == wanted_col[...]
        ).astype(jnp.float32).astype(jnp.bfloat16)
        across = (((0,), (0,)), ((), ()))
        slots = lax.dot_general(places, spread_v[...], across, preferred_element_type=jnp.float32)
        spread_shares = lax.dot_general(
            shares, spread_v[...], across, preferred_element_type=jnp.float32
        )
        relay_weights[s] = jnp.where(slots == wanted_row[...], spread_shares, 0.0).astype(
            jnp.bfloat16
        )

    def relay_sum(s, c):
        cols = columns(c, chunk)
        settle(relay_back.at[s, block(1, half - 1), cols], far_recv.at[s * chunks + c])
        tokens[s, :, cols] = jnp.dot(
            relay_weights[s], relay_back[s, :, cols], preferred_element_type=jnp.float32
        ).astype(jnp.bfloat16)
        remote(
            tokens.at[s, :, cols], far_sum.at[:, cols], sum_send.at[0], sum_recv.at[c], source_of(s)
        ).start()

    def on_relay(task):
        pl.when(relaying == 1)(task)

    def experts(g, halfway=None, between=None):
        rows = block(g * quarter, quarter)
        far = g >= 2
        s = g - 2

        @pl.loop(0, units // tile)
        def _(t):
            if halfway is not None:
                pl.when((relaying == 1) & (t == units // tile // 2))(halfway)
            if g == 0:
                load(gate_hbm, gate_v, gate_sem, t, tile).wait()
                load(up_hbm, up_v, up_sem, t, tile).wait()
            cols = columns(t, tile)
            x = arrived[rows, :]
            gate = jnp.dot(x, gate_v[:, cols], preferred_element_type=jnp.float32)
            up = jnp.dot(x, up_v[:, cols], preferred_element_type=jnp.float32)
            hidden[:, cols] = (gate / (1.0 + jnp.exp(-gate)) * up).astype(jnp.bfloat16)

        if between is not None:
            on_relay(between)

        @pl.loop(0, down_tiles)
        def _(t):
            step = g * down_tiles + t
            load_down(step).wait()
            cols = columns(t, down_tile)
            result = jnp.dot(
                hidden[...], down_v[step % depth], preferred_element_type=jnp.float32
            ).astype(jnp.bfloat16)
            arrived[rows, cols] = result
            if g == 0:
                near_back[block(0), cols] = result[:cap]

            if far:
                @pl.when(relaying == 1)
                def _():
                    relay_back[s, block(0), cols] = result[:cap]

            @pl.when(step + depth < 4 * down_tiles)
            def _():
                load_down(step + depth).start()

            if far:
                per = chunk // down_tile

                @pl.when(t % per == per - 1)
                def _():
                    c = t // per
                    wide = columns(c, chunk)

                    def give(p):
                        target = (1 + side) * quarter + flipped(spot, p, quarter)
                        place = pl.multiple_of((p + quarter * (1 - relaying)) * cap, cap)
                        remote(
                            arrived.at[block(g * quarter + p), wide],
                            relay_back.at[s, pl.ds(place, cap), wide],
                            far_send.at[s], far_recv.at[s * chunks + c], target,
                        ).start()

                    pl.when(relaying == 0)(functools.partial(give, 0))
                    for p in range(1, quarter):
                        give(p)

        if not far:
            for d in range(max(1, g * quarter), (g + 1) * quarter):
                remote(
                    arrived.at[block(d)], near_back.at[block(d)],
                    back_send.at[g], back_recv.at[g], flipped(me, d, n),
                ).start()

    def first_pick():
        read_meta(0)
        pick(0, 0)

    def second_pick():
        pick(0, chunks - 1)
        read_meta(1)

    on_relay(first_pick)
    own_rows.wait()
    settle(arrived.at[block(1, quarter - 1)], near_recv.at[0])
    experts(0, halfway=lambda: pick(0, 1), between=lambda: pick(0, 2))
    on_relay(second_pick)
    settle(arrived.at[block(quarter, quarter)], near_recv.at[1])
    experts(1, halfway=lambda: pick(1, 0), between=lambda: pick(1, 1))

    def await_far(s):
        first = half + s * quarter

        @pl.when(relaying == 1)
        def _():
            for c in range(chunks):
                cols = pl.ds(c * chunk, chunk)
                settle(arrived.at[block(first + 1, quarter - 1), cols], pick_recv.at[s * chunks + c])

        @pl.when(relaying == 0)
        def _():
            for c in range(chunks):
                cols = pl.ds(c * chunk, chunk)
                settle(arrived.at[block(first, quarter), cols], pick_recv.at[s * chunks + c])

    await_far(0)
    experts(2, halfway=lambda: pick(1, 2))
    on_relay(lambda: pick(1, chunks - 1))

    def relay_sums(s):
        @pl.loop(0, chunks)
        def _(c):
            relay_sum(s, c)

    on_relay(lambda: relay_sums(0))
    settle(near_back.at[block(1, quarter - 1)], back_recv.at[0])
    settle(near_back.at[block(quarter, quarter)], back_recv.at[1])

    @pl.loop(0, chunks)
    def _(c):
        cols = columns(c, chunk)
        total[:, cols] = jnp.dot(
            weights_v[...], near_back[:, cols], preferred_element_type=jnp.float32
        )

    await_far(1)
    experts(3)
    on_relay(lambda: relay_sums(1))
    stream_in.wait()
    for c in range(chunks):
        cols = pl.ds(c * chunk, chunk)
        settle(far_sum.at[:, cols], sum_recv.at[c])

    part = 32

    @pl.loop(0, total.shape[0] // part)
    def _(t):
        some = pl.ds(pl.multiple_of(t * part, part), part)
        combined = total[some, :] + far_sum[some, :].astype(jnp.float32)
        out_v[some, :] = (stream_v[some, :] + rms_scale(combined, gain_v[...])).astype(out_v.dtype)

    settle(normed_hbm, tok_send.at[0])
    settle(meta_hbm, meta_send.at[0])
    settle(rows_hbm.at[block(1, half - 1)], near_send.at[0])
    settle(arrived.at[block(1, quarter - 1)], back_send.at[0])
    settle(arrived.at[block(quarter, quarter)], back_send.at[1])

    @pl.when(relaying == 1)
    def _():
        for c in range(chunks):
            settle(picked.at[block(1, half - 1), pl.ds(c * chunk, chunk)], pick_send.at[c])
        settle(tokens, sum_send.at[0])
        for s in range(2):
            settle(arrived.at[block(half + s * quarter + 1, quarter - 1)], far_send.at[s])

    @pl.when(relaying == 0)
    def _():
        for s in range(2):
            settle(arrived.at[block(half + s * quarter, quarter)], far_send.at[s])


def run_experts(outgoing, normed, meta, w_gate, w_up, w_down, weights, stream, gain, n, cap):
    model_width, units = w_gate.shape[1], w_gate.shape[2]
    rows_blk = normed.shape[0]
    tile, down_tile, chunk, depth = 256, 256, model_width // 4, 4
    half, chunks = n // 2, 4
    total_rows = n * cap
    slots = np.arange(half * cap)
    spread = (slots[None, :] // cap == np.arange(half)[:, None]).astype(np.float32)
    wanted = (slots % cap + 1).astype(np.float32)
    constants = (
        jnp.asarray(spread, jnp.bfloat16),
        jnp.asarray(spread.T, jnp.bfloat16),
        jnp.asarray(wanted[None, :]),
        jnp.asarray(wanted[:, None]),
    )
    dma = pltpu.SemaphoreType.DMA
    vmem = pltpu.VMEM
    anywhere = pl.BlockSpec(memory_space=pl.ANY)
    near = pl.BlockSpec(memory_space=pltpu.VMEM)
    return pl.pallas_call(
        functools.partial(expert_kernel, n, cap, tile, down_tile, chunk),
        out_shape=jax.ShapeDtypeStruct(stream.shape, jnp.bfloat16),
        in_specs=[anywhere] * 6 + [near] * 5 + [anywhere, near],
        out_specs=near,
        scratch_shapes=[
            vmem((model_width, units), jnp.bfloat16),
            vmem((model_width, units), jnp.bfloat16),
            vmem((depth, units, down_tile), jnp.bfloat16),
            vmem((total_rows, model_width), jnp.bfloat16),
            vmem((n // 4 * cap, units), jnp.bfloat16),
            vmem((half * cap, model_width), jnp.bfloat16),
            vmem((rows_blk, model_width), jnp.bfloat16),
            vmem((2, rows_blk, model_width), jnp.bfloat16),
            vmem((half * cap, model_width), jnp.bfloat16),
            vmem((2, half * cap, model_width), jnp.bfloat16),
            vmem((2,) + meta.shape, jnp.float32),
            vmem((half * cap, rows_blk), jnp.bfloat16),
            vmem((2, rows_blk, half * cap), jnp.bfloat16),
            vmem(stream.shape, jnp.float32),
            vmem(stream.shape, jnp.float32),
            dma((units // tile,)),
            dma((units // tile,)),
            dma((depth,)),
            dma((1,)),
            dma((2 * chunks,)),
            dma((1,)),
            dma((2,)),
            dma((1,)),
            dma((2,)),
            dma((chunks,)),
            dma((2 * chunks,)),
            dma((2,)),
            dma((2,)),
            dma((2,)),
            dma((2 * chunks,)),
            dma((1,)),
            dma((chunks,)),
            dma((2,)),
        ],
        compiler_params=pltpu.CompilerParams(
            collective_id=0, has_side_effects=True, vmem_limit_bytes=67043328
        ),
        cost_estimate=pl.CostEstimate(
            flops=6 * total_rows * model_width * units,
            bytes_accessed=6 * model_width * units,
            transcendentals=total_rows * units,
        ),
    )(outgoing, normed, meta, w_gate, w_up, w_down, weights, *constants, stream, gain)


def per_device_whole(
    resid, gate_b, gate_c, value, taps, doc_ids, out_weight, norm_gains,
    routes, route_weights, w_gate, w_up, w_down,
):
    tok_dev = gate_b.shape[0]
    rows_blk, model_width = resid.shape
    experts = lax.axis_size("sp")
    capacity = max(2, 3 * TOP * rows_blk // (2 * experts))
    tap_reach = TAPS - 1
    product = gate_c.astype(jnp.float32) * value.astype(jnp.float32)
    id_values = doc_ids.astype(jnp.float32)
    id_row = jnp.pad(id_values[tok_dev - tap_reach :], (0, model_width - tap_reach))
    handed = passed_along(
        jnp.concatenate([product[tok_dev - tap_reach :], id_row[None]], axis=0), "sp", 1
    )
    ext_rows = jnp.concatenate([handed[:tap_reach], product], axis=0)
    ext_ids = jnp.concatenate([handed[tap_reach, :tap_reach], id_values], axis=0)
    tap_weights = taps.astype(jnp.float32)
    convolved = tap_weights[0] * product
    for distance in range(1, TAPS):
        earlier = ext_rows[tap_reach - distance : tap_reach - distance + tok_dev]
        same_doc = ext_ids[tap_reach - distance : tap_reach - distance + tok_dev] == id_values
        convolved = convolved + jnp.where(same_doc[:, None], tap_weights[distance] * earlier, 0.0)
    mixed_rows = (gate_b.astype(jnp.float32) * convolved).astype(jnp.bfloat16)
    projected = (
        jnp.dot(mixed_rows, out_weight, preferred_element_type=jnp.float32)
        .astype(jnp.bfloat16)
        .astype(jnp.float32)
    )
    stream = resid.astype(jnp.float32) + rms_scale(projected, norm_gains[0])
    normed = rms_scale(stream, norm_gains[1]).astype(jnp.bfloat16)

    def dot32(a, b):
        return jnp.dot(a, b, preferred_element_type=jnp.float32)

    me = lax.axis_index("sp")
    quarter, half = experts // 4, experts // 2
    plane = me // quarter
    far_relay = (2 - plane // 2) * quarter + me % quarter
    places = jnp.arange(half, dtype=jnp.int32)
    visited = jnp.concatenate([places ^ me, places ^ far_relay])
    names = routes[:, :, None] == visited[None, None, :]
    hit = jnp.any(names, axis=1)
    earlier_rows = jnp.asarray(np.tril(np.ones((rows_blk, rows_blk), np.float32), -1), jnp.bfloat16)
    rank = dot32(earlier_rows, hit.astype(jnp.bfloat16))
    place = jnp.where(hit, rank + 1.0, 0.0)
    slots = np.arange(half * capacity)
    spread = jnp.asarray(
        (slots[None, :] // capacity == np.arange(half)[:, None]).astype(np.float32), jnp.bfloat16
    )
    wanted = jnp.asarray((slots % capacity + 1).astype(np.float32))
    chosen = dot32(place[:, :half].astype(jnp.bfloat16), spread) == wanted[None, :]
    outgoing = lax.dot_general(
        chosen.astype(jnp.bfloat16),
        normed,
        (((0,), (0,)), ((), ())),
        preferred_element_type=jnp.float32,
    ).astype(jnp.bfloat16)
    shares = route_weights / jnp.sum(route_weights, axis=1, keepdims=True)
    share_of = jnp.sum(jnp.where(names, shares[:, :, None], 0.0), axis=1)
    weights = jnp.where(
        chosen, dot32(share_of[:, :half].astype(jnp.bfloat16), spread), 0.0
    ).astype(jnp.bfloat16)
    meta = jnp.concatenate([place[:, half:].T, share_of[:, half:].T], axis=0)
    return run_experts(
        outgoing, normed, meta, w_gate, w_up, w_down, weights, stream, norm_gains[2:3], experts, capacity
    )


def solution(mesh):
    experts = mesh.shape["sp"]
    whole_tokens = mesh.shape["tp"] == 1 and experts >= 8 and experts & (experts - 1) == 0
    per_device = per_device_whole if whole_tokens else per_device_split
    return jax.shard_map(
        per_device,
        mesh=mesh,
        in_specs=(
            P(("grp", "sp", "tp"), None),
            P(("grp", "sp"), "tp"),
            P(("grp", "sp"), "tp"),
            P(("grp", "sp"), "tp"),
            P(None, "tp"),
            P(("grp", "sp")),
            P("tp", None),
            P(),
            P(("grp", "sp"), None),
            P(("grp", "sp"), None),
            P("sp", None, "tp"),
            P("sp", None, "tp"),
            P("sp", "tp", None),
        ),
        out_specs=P(("grp", "sp", "tp"), None),
        check_vma=False,
    )
```

profile of v0, /device:TPU:0, one launch (start us, length us, event | category | flops | bytes accessed | tf_op | source)
XLA Modules:
  0.0 165.4 jit_solution(2721997845364644987)
XLA Ops:
  0.0 0.7 convert_element_type.47
  0.7 0.1 slice.59
  0.8 0.0 copy-start.8
  0.8 0.0 copy-start.11
  0.8 0.0 copy-start.9
  0.8 0.0 copy-start.10
  0.8 2.0 %convert_multiply_fusion.2 = f32[256,2048]{1,0:T(8,128)S(1)} fusion(bf16[256,2048]{1,0:T(8,128)(2,1)} %param.23, bf16[256,2048]{1,0:T(8,128)(2,1)} %param.22), kind=kLoop, calls=%fused_computation.21 | loop fusion | flops 1572864 | bytes 4194304 | tf_op jit(solution)/shard_map/mul | solution.py:531
  2.9 2.4 %collective-permute-start = (f32[3,2048]{1,0:T(4,128)S(1)}, f32[3,2048]{1,0:T(4,128)S(1)}, u32[]{:S(2)}, u32[]{:S(2)}) collective-permute-start(f32[3,2048]{1,0:T(4,128)S(1)} %pad_maximum_fusion.1), channel_id=1, source_target_pairs={{0,1},{1,2},{2,3},{3,4},{4,5},{5,6},{6,7},{7,8},{8,9},{9,10},{10,1... | collective-permute-start | bytes 73736 | tf_op jit(solution)/shard_map/ppermute | solution.py:21
  5.4 0.0 copy-done.6
  5.4 0.1 pad_add_fusion
  5.5 0.0 copy-done.7
  5.5 0.1 compare_reduce_fusion
  5.6 0.0 copy-done.3
  5.6 0.1 fusion.14
  5.7 0.1 fusion.22
  5.8 0.0 copy-done.4
  5.9 0.6 fusion.26
  6.5 0.3 convolution_compare_fusion
  6.8 0.9 fusion.12.weights_v
  7.7 0.6 pad_maximum_fusion.2.meta_hbm
  8.3 0.0 collective-permute-done
  8.3 0.1 pad_maximum_fusion.3
  8.4 0.1 slice_compare_fusion.1
  8.5 0.0 copy-start.2
  8.5 6.5 %fusion.7 = (f32[256]{0:T(256)S(1)}, bf16[256,2048]{1,0:T(8,128)(2,1)S(1)}) fusion(bf16[2048,2048]{1,0:T(8,128)(2,1)} %param.26, f32[2,2048]{1,0:T(2,128)S(1)} %slice.79, f32[256,2048]{1,0:T(8,128)S(1)} %convert_multiply_fusion.2, bf16[256,2048]{1,0:T(8,128)(2,1)S(1)} %copy-done.10, f32[2048]{0:T(1024)S(1)} %bitcast.28, f32[2048]{0:T(1024)S(1)} %bitcast.27, ...), kind=kOutput, calls=%fused_computation.13 | convolution fusion | flops 2155872000 | bytes 12625408 | tf_op jit(solution)/shard_map/dot_general | solution.py:547
  15.0 0.6 multiply_reduce_fusion
  15.7 0.2 multiply_convert_fusion.normed_hbm
  15.9 0.0 copy-start.1
  15.9 1.2 copy-done.1
  17.1 1.8 %convolution_convert_fusion.rows_hbm = bf16[384,2048]{1,0:T(8,128)(2,1)} fusion(pred[256,384]{1,0:T(32,128)(4,1)S(1)} %convolution_compare_fusion, bf16[256,2048]{1,0:T(8,128)(2,1)S(1)} %multiply_convert_fusion.normed_hbm), kind=kOutput, calls=%fused_computation | convolution fusion | flops 403439616 | bytes 2719744 | tf_op jit(solution)/shard_map/dot_general | solution.py:574
  18.9 144.2 %shard_map.190 = bf16[256,2048]{1,0:T(8,128)(2,1)} custom-call(bf16[384,2048]{1,0:T(8,128)(2,1)} %convolution_convert_fusion.rows_hbm, bf16[256,2048]{1,0:T(8,128)(2,1)} %copy-done.1, f32[16,256]{1,0:T(8,128)} %pad_maximum_fusion.2.meta_hbm, bf16[1,2048,4096]{2,1,0:T(8,128)(2,1)} %gate_hbm.1, bf16[1,2048,4096]{2,1,0:T(8,128)(2,1)} %up_hbm.1, ...), custom_call_target="tpu_custom_call" | custom-call | flops 38654705664 | bytes 50331648 | tf_op jit(solution)/shard_map/pallas_call | solution.py:471
  163.1 2.3 %copy.27 = bf16[256,2048]{1,0:T(8,128)(2,1)} copy(bf16[256,2048]{1,0:T(8,128)(2,1)} %shard_map.190) | data formatting | bytes 2097152
  (26 shorter events, 0.1 us)
Async XLA Ops:
  0.8 4.6 %copy-start.6 = (f32[256,2]{0,1:T(2,128)S(1)}, f32[256,2]{0,1:T(2,128)}, u32[]{:S(2)}) copy-start(f32[256,2]{0,1:T(2,128)} %param.29) | copy-start | bytes 6148
  0.8 4.7 %copy-start.7 = (s32[256,2]{0,1:T(2,128)S(1)}, s32[256,2]{0,1:T(2,128)}, u32[]{:S(2)}) copy-start(s32[256,2]{0,1:T(2,128)} %param.28) | copy-start | bytes 6148
  0.8 4.8 %copy-start.3 = (bf16[256,256]{1,0:T(8,128)(2,1)S(1)}, bf16[256,256]{1,0:T(8,128)(2,1)}, u32[]{:S(2)}) copy-start(bf16[256,256]{1,0:T(8,128)(2,1)} %constant.65.clone) | copy-start | bytes 393220
  0.8 5.0 %copy-start.4 = (bf16[3,2048]{1,0:T(4,128)(2,1)S(1)}, bf16[3,2048]{1,0:T(4,128)(2,1)}, u32[]{:S(2)}) copy-start(bf16[3,2048]{1,0:T(4,128)(2,1)} %param.24) | copy-start | bytes 36868
  0.8 5.1 %copy-start.5 = (f32[3,2048]{1,0:T(4,128)S(1)}, f32[3,2048]{1,0:T(4,128)}, u32[]{:S(2)}) copy-start(f32[3,2048]{1,0:T(4,128)} %param.27) | copy-start | bytes 73732
  0.8 5.7 %copy-start.8 = (bf16[8,384]{1,0:T(8,128)(2,1)S(1)}, bf16[8,384]{1,0:T(8,128)(2,1)}, u32[]{:S(2)}) copy-start(bf16[8,384]{1,0:T(8,128)(2,1)} %constant.66.clone.spread_v) | copy-start | bytes 18436
  0.8 5.7 %copy-start.11 = (f32[384]{0:T(512)S(1)}, f32[384]{0:T(512)}, u32[]{:S(2)}) copy-start(f32[384]{0:T(512)} %constant.67.clone) | copy-start | bytes 4612
  0.8 7.6 %copy-start.9 = (s32[256]{0:T(256)S(1)}, s32[256]{0:T(256)}, u32[]{:S(2)}) copy-start(s32[256]{0:T(256)} %param.25) | copy-start | bytes 3076
  0.8 7.7 %copy-start.10 = (bf16[256,2048]{1,0:T(8,128)(2,1)S(1)}, bf16[256,2048]{1,0:T(8,128)(2,1)}, u32[]{:S(2)}) copy-start(bf16[256,2048]{1,0:T(8,128)(2,1)} %param.21) | copy-start | bytes 3145732
  2.9 5.4 %collective-permute-start = (f32[3,2048]{1,0:T(4,128)S(1)}, f32[3,2048]{1,0:T(4,128)S(1)}, u32[]{:S(2)}, u32[]{:S(2)}) collective-permute-start(f32[3,2048]{1,0:T(4,128)S(1)} %pad_maximum_fusion.1), channel_id=1, source_target_pairs={{0,1},{1,2},{2,3},{3,4},{4,5},{5,6},{6,7},{7,8},{8,9},{9,10},{10,1... | collective-permute-start | bytes 73736 | tf_op jit(solution)/shard_map/ppermute | solution.py:21
  8.5 6.5 %copy-start.2 = (bf16[256,2048]{1,0:T(8,128)(2,1)S(1)}, bf16[256,2048]{1,0:T(8,128)(2,1)}, u32[]{:S(2)}) copy-start(bf16[256,2048]{1,0:T(8,128)(2,1)} %param.20) | copy-start | bytes 3145732
  15.7 3.2 %copy-start = (f32[256,2048]{1,0:T(8,128)}, f32[256,2048]{1,0:T(8,128)S(1)}, u32[]{:S(2)}) copy-start(f32[256,2048]{1,0:T(8,128)S(1)} %get-tuple-element.6.stream_hbm) | copy-start | bytes 6291460
  15.9 1.2 copy-start.1
where the time goes:
time: 166 us; the launch traced here: 165 us
  Pallas kernels  144 us (87%)
  matrix products  9.61 us (6%)
  other arithmetic  4.62 us (3%)
  local copies, waits for them, and re-layouts  4.28 us (3%)
  starting transfers between devices  2.4 us (1%)
    pallas_call x1, Pallas kernels, run_experts(): pl.pallas_call(functools.partial(expert_kernel, n, cap, tile, down_tile,...  144 us
    dot_general x1, matrix products, per_device_whole(): jnp.dot(mixed_rows, out_weight, preferred_element_type=jnp.float32)  6.5 us
    unnamed x25, local copies, waits for them, and re-layouts  3.53 us
  transfers between devices with their start and end apart: 1, of which 0 were waited for; matrix products, arithmetic and copies ran while one was open for 2% of the time, Pallas kernels for 0%

commit v1 on v0

--- a/solution.py
+++ b/solution.py
@@ -141,6 +141,11 @@
     return out
 
 
+def pass_plan(n):
+    quarter, half = n // 4, n // 2
+    return [(range(quarter), None), ((), 0), (range(quarter, half), None), ((), 1)]
+
+
 def expert_kernel(
     n, cap, tile, down_tile, chunk,
     rows_hbm, normed_hbm, meta_hbm, gate_hbm, up_hbm, down_hbm,
@@ -162,10 +167,10 @@
     chunks = width // chunk
     down_tiles = width // down_tile
     far_relay = (2 - side) * quarter + spot
-    my_turn = 1 - relaying
+    my_turn = relaying
 
     def source_of(s):
-        return ((2 - side) + s * (1 - 2 * side)) * quarter + spot
+        return (3 - s - (3 - 2 * s) * side) * quarter + spot
 
     def columns(t, size):
         return pl.ds(pl.multiple_of(t * size, size), size)
@@ -193,7 +198,21 @@
     def block(i, count=1):
         return pl.ds(i * cap, count * cap)
 
+    passes = pass_plan(n)
+    pass_starts, places, first_far = [0], {}, {}
+    for members, group in passes:
+        for d in members:
+            places[d] = pass_starts[-1] + d - members[0]
+        end = pass_starts[-1] + len(members)
+        if group is not None:
+            first_far[group] = end
+            end += quarter
+        pass_starts.append(end)
+
     barrier = pltpu.get_barrier_semaphore()
+
+    def on_edge(task):
+        pl.when(relaying == 0)(task)
 
     def greet(device):
         pl.semaphore_signal(barrier, inc=1, device_id={"sp": device}, device_id_type=MESH)
@@ -232,19 +251,14 @@
     def send_near(distances):
         for d in distances:
             remote(
-                rows_hbm.at[block(d)], arrived.at[block(d)],
+                rows_hbm.at[block(d)], arrived.at[block(places[d])],
                 near_send.at[0], near_recv.at[d // quarter], flipped(me, d, n),
             ).start()
 
-    @pl.when(relaying == 1)
-    def _():
-        send_tokens()
-
-    send_near(list(range(1, quarter)) + list(range(quarter, half)))
-
-    @pl.when(relaying == 0)
-    def _():
-        send_tokens()
+    middle = quarter + quarter // 2
+    send_tokens()
+    send_near(range(1, middle))
+    on_edge(lambda: send_near(range(middle, half)))
 
     def pick(s, c):
         cols = columns(c, chunk)
@@ -254,12 +268,12 @@
         rows = jnp.dot(
             chosen_t[...], tokens[s, :, cols], preferred_element_type=jnp.float32
         ).astype(jnp.bfloat16)
-        arrived[block(half + s * quarter), cols] = rows[:cap]
+        arrived[block(first_far[s]), cols] = rows[:cap]
         picked[pl.ds(cap, (half - 1) * cap), cols] = rows[cap:]
         for d in list(range(quarter, half)) + list(range(1, quarter)):
             remote(
                 picked.at[block(d), cols],
-                arrived.at[block(half + s * quarter + d % quarter), cols],
+                arrived.at[block(first_far[s] + d % quarter), cols],
                 pick_send.at[c], pick_recv.at[s * chunks + c], flipped(me, d, n),
             ).start()
 
@@ -292,15 +306,20 @@
     def on_relay(task):
         pl.when(relaying == 1)(task)
 
-    def experts(g, halfway=None, between=None):
-        rows = block(g * quarter, quarter)
-        far = g >= 2
-        s = g - 2
+    def experts(g, amid=(), between=None, amid_down=()):
+        first, after = pass_starts[g], pass_starts[g + 1]
+        rows = block(first, after - first)
+        used = pl.ds(0, (after - first) * cap)
+        s = passes[g][1]
+        far = s is not None
+        own_far = len(passes[g][0]) * cap
+        has_own = 0 in passes[g][0]
 
         @pl.loop(0, units // tile)
         def _(t):
-            if halfway is not None:
-                pl.when((relaying == 1) & (t == units // tile // 2))(halfway)
+            for when, role, task in amid:
+                here = (t == when) if role is None else (relaying == role) & (t == when)
+                pl.when(here)(task)
             if g == 0:
                 load(gate_hbm, gate_v, gate_sem, t, tile).wait()
                 load(up_hbm, up_v, up_sem, t, tile).wait()
@@ -308,29 +327,32 @@
             x = arrived[rows, :]
             gate = jnp.dot(x, gate_v[:, cols], preferred_element_type=jnp.float32)
             up = jnp.dot(x, up_v[:, cols], preferred_element_type=jnp.float32)
-            hidden[:, cols] = (gate / (1.0 + jnp.exp(-gate)) * up).astype(jnp.bfloat16)
+            hidden[used, cols] = (gate / (1.0 + jnp.exp(-gate)) * up).astype(jnp.bfloat16)
 
         if between is not None:
-            on_relay(between)
+            between()
 
         @pl.loop(0, down_tiles)
         def _(t):
             step = g * down_tiles + t
+            for when, role, task in amid_down:
+                here = (t == when) if role is None else (relaying == role) & (t == when)
+                pl.when(here)(task)
             load_down(step).wait()
             cols = columns(t, down_tile)
             result = jnp.dot(
-                hidden[...], down_v[step % depth], preferred_element_type=jnp.float32
+                hidden[used, :], down_v[step % depth], preferred_element_type=jnp.float32
             ).astype(jnp.bfloat16)
             arrived[rows, cols] = result
-            if g == 0:
+            if has_own:
                 near_back[block(0), cols] = result[:cap]
 
             if far:
                 @pl.when(relaying == 1)
                 def _():
-                    relay_back[s, block(0), cols] = result[:cap]
-
-            @pl.when(step + depth < 4 * down_tiles)
+                    relay_back[s, block(0), cols] = result[own_far:own_far + cap]
+
+            @pl.when(step + depth < len(passes) * down_tiles)
             def _():
                 load_down(step + depth).start()
 
@@ -340,46 +362,60 @@
                 @pl.when(t % per == per - 1)
                 def _():
                     c = t // per
-                    wide = columns(c, chunk)
-
-                    def give(p):
-                        target = (1 + side) * quarter + flipped(spot, p, quarter)
-                        place = pl.multiple_of((p + quarter * (1 - relaying)) * cap, cap)
-                        remote(
-                            arrived.at[block(g * quarter + p), wide],
-                            relay_back.at[s, pl.ds(place, cap), wide],
-                            far_send.at[s], far_recv.at[s * chunks + c], target,
-                        ).start()
-
-                    pl.when(relaying == 0)(functools.partial(give, 0))
-                    for p in range(1, quarter):
-                        give(p)
-
-        if not far:
-            for d in range(max(1, g * quarter), (g + 1) * quarter):
-                remote(
-                    arrived.at[block(d)], near_back.at[block(d)],
-                    back_send.at[g], back_recv.at[g], flipped(me, d, n),
-                ).start()
+                    if s == 0:
+                        on_edge(lambda: give_far(s, c, range(quarter)))
+                    else:
+                        on_edge(lambda: give_far(s, c, range(1)))
+                        give_far(s, c, range(1, quarter))
+
+    def give_far(s, c, spots):
+        wide = columns(c, chunk)
+        for p in spots:
+            target = (1 + side) * quarter + flipped(spot, p, quarter)
+            place = pl.multiple_of((p + quarter * (1 - relaying)) * cap, cap)
+            remote(
+                arrived.at[block(first_far[s] + p), wide],
+                relay_back.at[s, pl.ds(place, cap), wide],
+                far_send.at[s], far_recv.at[s * chunks + c], target,
+            ).start()
+
+    def near_distances(i):
+        return range(max(1, i * quarter), (i + 1) * quarter)
+
+    def near_part(ref, i, places):
+        members = near_distances(i)
+        return ref.at[block(places[members[0]], len(members))]
+
+    def give_near(distances):
+        for d in distances:
+            i = d // quarter
+            remote(
+                arrived.at[block(places[d])], near_back.at[block(d)],
+                back_send.at[i], back_recv.at[i], flipped(me, d, n),
+            ).start()
+
+    plain = {d: d for d in range(half)}
 
     def first_pick():
         read_meta(0)
         pick(0, 0)
 
-    def second_pick():
-        pick(0, chunks - 1)
-        read_meta(1)
-
     on_relay(first_pick)
     own_rows.wait()
-    settle(arrived.at[block(1, quarter - 1)], near_recv.at[0])
-    experts(0, halfway=lambda: pick(0, 1), between=lambda: pick(0, 2))
-    on_relay(second_pick)
-    settle(arrived.at[block(quarter, quarter)], near_recv.at[1])
-    experts(1, halfway=lambda: pick(1, 0), between=lambda: pick(1, 1))
+    settle(near_part(arrived, 0, places), near_recv.at[0])
+    experts(
+        0, amid=[(8, 1, lambda: pick(0, 1))],
+        amid_down=[(0, 1, lambda: pick(0, 2))],
+    )
+
+    def last_of_first():
+        pick(0, chunks - 1)
+        send_near(range(middle, half))
+
+    on_relay(last_of_first)
 
     def await_far(s):
-        first = half + s * quarter
+        first = first_far[s]
 
         @pl.when(relaying == 1)
         def _():
@@ -393,18 +429,41 @@
                 cols = pl.ds(c * chunk, chunk)
                 settle(arrived.at[block(first, quarter), cols], pick_recv.at[s * chunks + c])
 
+    def first_of_second():
+        read_meta(1)
+        pick(1, 0)
+
     await_far(0)
-    experts(2, halfway=lambda: pick(1, 2))
-    on_relay(lambda: pick(1, chunks - 1))
+    experts(
+        1, amid=[(5, 1, first_of_second), (14, 1, lambda: pick(1, 1))],
+        amid_down=[(6, 1, lambda: pick(1, 2))],
+    )
+    def last_of_second():
+        pick(1, chunks - 1)
+        for c in range(chunks):
+            give_far(0, c, range(1, quarter))
+
+    settle(near_part(arrived, 1, places), near_recv.at[1])
+    experts(
+        2, amid=[
+            (1, 1, last_of_second), (12, 1, lambda: relay_sum(0, 0)),
+            (15, 1, lambda: relay_sum(0, 1)),
+        ],
+        amid_down=[(4, 1, lambda: relay_sum(0, 2))],
+    )
+    on_relay(lambda: relay_sum(0, 3))
 
     def relay_sums(s):
         @pl.loop(0, chunks)
         def _(c):
             relay_sum(s, c)
 
-    on_relay(lambda: relay_sums(0))
-    settle(near_back.at[block(1, quarter - 1)], back_recv.at[0])
-    settle(near_back.at[block(quarter, quarter)], back_recv.at[1])
+    await_far(1)
+    experts(3, amid=[(7, None, lambda: give_near(range(middle, half)))])
+    give_near(range(1, middle))
+    on_relay(lambda: relay_sums(1))
+    for i in range(2):
+        settle(near_part(near_back, i, plain), back_recv.at[i])
 
     @pl.loop(0, chunks)
     def _(c):
@@ -413,9 +472,6 @@
             weights_v[...], near_back[:, cols], preferred_element_type=jnp.float32
         )
 
-    await_far(1)
-    experts(3)
-    on_relay(lambda: relay_sums(1))
     stream_in.wait()
     for c in range(chunks):
         cols = pl.ds(c * chunk, chunk)
@@ -432,8 +488,8 @@
     settle(normed_hbm, tok_send.at[0])
     settle(meta_hbm, meta_send.at[0])
     settle(rows_hbm.at[block(1, half - 1)], near_send.at[0])
-    settle(arrived.at[block(1, quarter - 1)], back_send.at[0])
-    settle(arrived.at[block(quarter, quarter)], back_send.at[1])
+    for i in range(2):
+        settle(near_part(arrived, i, places), back_send.at[i])
 
     @pl.when(relaying == 1)
     def _():
@@ -441,12 +497,12 @@
             settle(picked.at[block(1, half - 1), pl.ds(c * chunk, chunk)], pick_send.at[c])
         settle(tokens, sum_send.at[0])
         for s in range(2):
-            settle(arrived.at[block(half + s * quarter + 1, quarter - 1)], far_send.at[s])
+            settle(arrived.at[block(first_far[s] + 1, quarter - 1)], far_send.at[s])
 
     @pl.when(relaying == 0)
     def _():
         for s in range(2):
-            settle(arrived.at[block(half + s * quarter, quarter)], far_send.at[s])
+            settle(arrived.at[block(first_far[s], quarter)], far_send.at[s])
 
 
 def run_experts(outgoing, normed, meta, w_gate, w_up, w_down, weights, stream, gain, n, cap):
@@ -455,6 +511,7 @@
     tile, down_tile, chunk, depth = 256, 256, model_width // 4, 4
     half, chunks = n // 2, 4
     total_rows = n * cap
+    longest = max(len(m) + (0 if s is None else n // 4) for m, s in pass_plan(n))
     slots = np.arange(half * cap)
     spread = (slots[None, :] // cap == np.arange(half)[:, None]).astype(np.float32)
     wanted = (slots % cap + 1).astype(np.float32)
@@ -478,7 +535,7 @@
             vmem((model_width, units), jnp.bfloat16),
             vmem((depth, units, down_tile), jnp.bfloat16),
             vmem((total_rows, model_width), jnp.bfloat16),
-            vmem((n // 4 * cap, units), jnp.bfloat16),
+            vmem((longest * cap, units), jnp.bfloat16),
             vmem((half * cap, model_width), jnp.bfloat16),
             vmem((rows_blk, model_width), jnp.bfloat16),
             vmem((2, rows_blk, model_width), jnp.bfloat16),
@@ -497,11 +554,11 @@
             dma((1,)),
             dma((2,)),
             dma((1,)),
-            dma((2,)),
+            dma((3,)),
             dma((chunks,)),
             dma((2 * chunks,)),
-            dma((2,)),
-            dma((2,)),
+            dma((3,)),
+            dma((3,)),
             dma((2,)),
             dma((2 * chunks,)),
             dma((1,)),

time: 166 us -> 141 us (0.85)
  the two profiles are of different devices: /device:TPU:0 before, /device:TPU:10 now
where the time goes in v1:
time: 141 us
  Pallas kernels  120 us (85%)
  matrix products  9.61 us (7%)
  other arithmetic  4.62 us (3%)
  local copies, waits for them, and re-layouts  4.28 us (3%)
  starting transfers between devices  1.92 us (1%)
    pallas_call x1, Pallas kernels, run_experts(): pl.pallas_call(functools.partial(expert_kernel, n, cap, tile, down_tile,...  120 us
    dot_general x1, matrix products, per_device_whole(): jnp.dot(mixed_rows, out_weight, preferred_element_type=jnp.float32)  6.5 us
    unnamed x25, local copies, waits for them, and re-layouts  3.53 us
  transfers between devices with their start and end apart: 1, of which 1 were waited for; matrix products, arithmetic and copies ran while one was open for 2% of the time, Pallas kernels for 0%

profile of v1, /device:TPU:10, one launch (start us, length us, event | category | flops | bytes accessed | tf_op | source)
XLA Modules:
  0.0 140.8 jit_solution(15872369355547069531)
XLA Ops:
  0.0 0.7 convert_element_type.47
  0.7 0.1 slice.59
  0.8 0.0 copy-start.8
  0.8 0.0 copy-start.11
  0.8 0.0 copy-start.9
  0.8 0.0 copy-start.10
  0.8 2.0 %convert_multiply_fusion.2 = f32[256,2048]{1,0:T(8,128)S(1)} fusion(bf16[256,2048]{1,0:T(8,128)(2,1)} %param.23, bf16[256,2048]{1,0:T(8,128)(2,1)} %param.22), kind=kLoop, calls=%fused_computation.21 | loop fusion | flops 1572864 | bytes 4194304 | tf_op jit(solution)/shard_map/mul | solution.py:588
  2.9 1.9 %collective-permute-start = (f32[3,2048]{1,0:T(4,128)S(1)}, f32[3,2048]{1,0:T(4,128)S(1)}, u32[]{:S(2)}, u32[]{:S(2)}) collective-permute-start(f32[3,2048]{1,0:T(4,128)S(1)} %pad_maximum_fusion.1), channel_id=1, source_target_pairs={{0,1},{1,2},{2,3},{3,4},{4,5},{5,6},{6,7},{7,8},{8,9},{9,10},{10,1... | collective-permute-start | bytes 73736 | tf_op jit(solution)/shard_map/ppermute | solution.py:21
  4.9 0.0 copy-done.6
  4.9 0.1 pad_add_fusion
  5.0 0.1 compare_reduce_fusion
  5.1 0.0 copy-done.3
  5.1 0.1 fusion.14
  5.3 0.1 fusion.22
  5.4 0.0 copy-done.5
  5.4 0.6 fusion.26
  6.0 0.0 copy-done.8
  6.0 0.3 convolution_compare_fusion
  6.3 0.9 fusion.12.weights_v
  7.2 0.6 pad_maximum_fusion.2.meta_hbm
  7.8 0.3 collective-permute-done
  8.1 0.1 pad_maximum_fusion.3
  8.2 0.1 slice_compare_fusion.1
  8.3 0.0 copy-start.2
  8.3 6.5 %fusion.7 = (f32[256]{0:T(256)S(1)}, bf16[256,2048]{1,0:T(8,128)(2,1)S(1)}) fusion(bf16[2048,2048]{1,0:T(8,128)(2,1)} %param.26, f32[2,2048]{1,0:T(2,128)S(1)} %slice.79, f32[256,2048]{1,0:T(8,128)S(1)} %convert_multiply_fusion.2, bf16[256,2048]{1,0:T(8,128)(2,1)S(1)} %copy-done.10, f32[2048]{0:T(1024)S(1)} %bitcast.28, f32[2048]{0:T(1024)S(1)} %bitcast.27, ...), kind=kOutput, calls=%fused_computation.13 | convolution fusion | flops 2155872000 | bytes 12625408 | tf_op jit(solution)/shard_map/dot_general | solution.py:604
  14.9 0.6 multiply_reduce_fusion
  15.5 0.2 multiply_convert_fusion.normed_hbm
  15.8 0.0 copy-start.1
  15.8 1.2 copy-done.1
  16.9 1.8 %convolution_convert_fusion.rows_hbm = bf16[384,2048]{1,0:T(8,128)(2,1)} fusion(pred[256,384]{1,0:T(32,128)(4,1)S(1)} %convolution_compare_fusion, bf16[256,2048]{1,0:T(8,128)(2,1)S(1)} %multiply_convert_fusion.normed_hbm), kind=kOutput, calls=%fused_computation | convolution fusion | flops 403439616 | bytes 2719744 | tf_op jit(solution)/shard_map/dot_general | solution.py:631
  18.7 119.8 %shard_map.190 = bf16[256,2048]{1,0:T(8,128)(2,1)} custom-call(bf16[384,2048]{1,0:T(8,128)(2,1)} %convolution_convert_fusion.rows_hbm, bf16[256,2048]{1,0:T(8,128)(2,1)} %copy-done.1, f32[16,256]{1,0:T(8,128)} %pad_maximum_fusion.2.meta_hbm, bf16[1,2048,4096]{2,1,0:T(8,128)(2,1)} %gate_hbm.1, bf16[1,2048,4096]{2,1,0:T(8,128)(2,1)} %up_hbm.1, ...), custom_call_target="tpu_custom_call" | custom-call | flops 38654705664 | bytes 50331648 | tf_op jit(solution)/shard_map/pallas_call | solution.py:528
  138.5 2.3 %copy.27 = bf16[256,2048]{1,0:T(8,128)(2,1)} copy(bf16[256,2048]{1,0:T(8,128)(2,1)} %shard_map.190) | data formatting | bytes 2097152
  (26 shorter events, 0.1 us)
Async XLA Ops:
  0.8 4.1 %copy-start.6 = (f32[256,2]{0,1:T(2,128)S(1)}, f32[256,2]{0,1:T(2,128)}, u32[]{:S(2)}) copy-start(f32[256,2]{0,1:T(2,128)} %param.29) | copy-start | bytes 6148
  0.8 4.3 %copy-start.7 = (s32[256,2]{0,1:T(2,128)S(1)}, s32[256,2]{0,1:T(2,128)}, u32[]{:S(2)}) copy-start(s32[256,2]{0,1:T(2,128)} %param.28) | copy-start | bytes 6148
  0.8 4.3 %copy-start.3 = (bf16[256,256]{1,0:T(8,128)(2,1)S(1)}, bf16[256,256]{1,0:T(8,128)(2,1)}, u32[]{:S(2)}) copy-start(bf16[256,256]{1,0:T(8,128)(2,1)} %constant.65.clone) | copy-start | bytes 393220
  0.8 4.6 %copy-start.4 = (bf16[3,2048]{1,0:T(4,128)(2,1)S(1)}, bf16[3,2048]{1,0:T(4,128)(2,1)}, u32[]{:S(2)}) copy-start(bf16[3,2048]{1,0:T(4,128)(2,1)} %param.24) | copy-start | bytes 36868
  0.8 4.6 %copy-start.5 = (f32[3,2048]{1,0:T(4,128)S(1)}, f32[3,2048]{1,0:T(4,128)}, u32[]{:S(2)}) copy-start(f32[3,2048]{1,0:T(4,128)} %param.27) | copy-start | bytes 73732
  0.8 5.3 %copy-start.8 = (bf16[8,384]{1,0:T(8,128)(2,1)S(1)}, bf16[8,384]{1,0:T(8,128)(2,1)}, u32[]{:S(2)}) copy-start(bf16[8,384]{1,0:T(8,128)(2,1)} %constant.66.clone.spread_v) | copy-start | bytes 18436
  0.8 5.2 %copy-start.11 = (f32[384]{0:T(512)S(1)}, f32[384]{0:T(512)}, u32[]{:S(2)}) copy-start(f32[384]{0:T(512)} %constant.67.clone) | copy-start | bytes 4612
  0.8 7.4 %copy-start.9 = (s32[256]{0:T(256)S(1)}, s32[256]{0:T(256)}, u32[]{:S(2)}) copy-start(s32[256]{0:T(256)} %param.25) | copy-start | bytes 3076
  0.8 7.5 %copy-start.10 = (bf16[256,2048]{1,0:T(8,128)(2,1)S(1)}, bf16[256,2048]{1,0:T(8,128)(2,1)}, u32[]{:S(2)}) copy-start(bf16[256,2048]{1,0:T(8,128)(2,1)} %param.21) | copy-start | bytes 3145732
  2.9 5.2 %collective-permute-start = (f32[3,2048]{1,0:T(4,128)S(1)}, f32[3,2048]{1,0:T(4,128)S(1)}, u32[]{:S(2)}, u32[]{:S(2)}) collective-permute-start(f32[3,2048]{1,0:T(4,128)S(1)} %pad_maximum_fusion.1), channel_id=1, source_target_pairs={{0,1},{1,2},{2,3},{3,4},{4,5},{5,6},{6,7},{7,8},{8,9},{9,10},{10,1... | collective-permute-start | bytes 73736 | tf_op jit(solution)/shard_map/ppermute | solution.py:21
  8.3 6.5 %copy-start.2 = (bf16[256,2048]{1,0:T(8,128)(2,1)S(1)}, bf16[256,2048]{1,0:T(8,128)(2,1)}, u32[]{:S(2)}) copy-start(bf16[256,2048]{1,0:T(8,128)(2,1)} %param.20) | copy-start | bytes 3145732
  15.5 3.2 %copy-start = (f32[256,2048]{1,0:T(8,128)}, f32[256,2048]{1,0:T(8,128)S(1)}, u32[]{:S(2)}) copy-start(f32[256,2048]{1,0:T(8,128)S(1)} %get-tuple-element.6.stream_hbm) | copy-start | bytes 6291460
  15.8 1.2 copy-start.1

commit v2 on v1

--- a/solution.py
+++ b/solution.py
@@ -148,10 +148,10 @@
 
 def expert_kernel(
     n, cap, tile, down_tile, chunk,
-    rows_hbm, normed_hbm, meta_hbm, gate_hbm, up_hbm, down_hbm,
-    weights_v, spread_v, spread_t, wanted_row, wanted_col, stream_hbm, gain_v, out_v,
-    gate_v, up_v, down_v, arrived, hidden, near_back, far_sum, tokens, picked, relay_back,
-    meta_v, chosen_t, relay_weights, stream_v, total,
+    normed_hbm, meta_hbm, gate_hbm, up_hbm, down_hbm,
+    near_meta, spread_v, spread_t, wanted_row, wanted_col, stream_hbm, gain_v, out_v,
+    gate_v, up_v, down_v, arrived, hidden, near_rows, near_back, far_sum, tokens, picked, relay_back,
+    meta_v, chosen_t, near_weights, relay_weights, stream_v, total,
     gate_sem, up_sem, down_sem, tok_send, tok_recv, meta_send, meta_recv,
     near_send, near_recv, pick_send, pick_recv, back_send, back_recv,
     far_send, far_recv, sum_send, sum_recv, own_sem,
@@ -226,8 +226,26 @@
         greet(source_of(0))
         greet(source_of(1))
 
-    own_rows = pltpu.make_async_copy(rows_hbm.at[block(0)], arrived.at[block(0)], own_sem.at[0])
-    own_rows.start()
+    normed_in = pltpu.make_async_copy(normed_hbm, far_sum, own_sem.at[0])
+    normed_in.start()
+
+    def select(meta, weights_ref):
+        places = meta[:half].astype(jnp.bfloat16)
+        shares = meta[half:].astype(jnp.bfloat16)
+        chosen_t[...] = (
+            jnp.dot(spread_t[...], places, preferred_element_type=jnp.float32) == wanted_col[...]
+        ).astype(jnp.float32).astype(jnp.bfloat16)
+        across = (((0,), (0,)), ((), ()))
+        slots = lax.dot_general(places, spread_v[...], across, preferred_element_type=jnp.float32)
+        spread_shares = lax.dot_general(
+            shares, spread_v[...], across, preferred_element_type=jnp.float32
+        )
+        weights_ref[...] = jnp.where(slots == wanted_row[...], spread_shares, 0.0).astype(
+            jnp.bfloat16
+        )
+
+    select(near_meta[...], near_weights)
+    normed_in.wait()
     for t in range(units // tile):
         load(gate_hbm, gate_v, gate_sem, t, tile).start()
         load(up_hbm, up_v, up_sem, t, tile).start()
@@ -235,6 +253,16 @@
         load_down(t).start()
     stream_in = pltpu.make_async_copy(stream_hbm, stream_v, own_sem.at[1])
     stream_in.start()
+
+    @pl.loop(0, chunks)
+    def _(c):
+        cols = columns(c, chunk)
+        rows = jnp.dot(
+            chosen_t[...], far_sum[:, cols], preferred_element_type=jnp.float32
+        ).astype(jnp.bfloat16)
+        arrived[block(0), cols] = rows[:cap]
+        near_rows[:, cols] = rows[cap:]
+
     pl.semaphore_wait(barrier, half + 2 * relaying)
 
     def send_tokens():
@@ -251,7 +279,7 @@
     def send_near(distances):
         for d in distances:
             remote(
-                rows_hbm.at[block(d)], arrived.at[block(places[d])],
+                near_rows.at[block(d - 1)], arrived.at[block(places[d])],
                 near_send.at[0], near_recv.at[d // quarter], flipped(me, d, n),
             ).start()
 
@@ -279,19 +307,7 @@
 
     def read_meta(s):
         settle(meta_v.at[s], meta_recv.at[s])
-        places = meta_v[s, :half].astype(jnp.bfloat16)
-        shares = meta_v[s, half:].astype(jnp.bfloat16)
-        chosen_t[...] = (
-            jnp.dot(spread_t[...], places, preferred_element_type=jnp.float32) == wanted_col[...]
-        ).astype(jnp.float32).astype(jnp.bfloat16)
-        across = (((0,), (0,)), ((), ()))
-        slots = lax.dot_general(places, spread_v[...], across, preferred_element_type=jnp.float32)
-        spread_shares = lax.dot_general(
-            shares, spread_v[...], across, preferred_element_type=jnp.float32
-        )
-        relay_weights[s] = jnp.where(slots == wanted_row[...], spread_shares, 0.0).astype(
-            jnp.bfloat16
-        )
+        select(meta_v[s], relay_weights.at[s])
 
     def relay_sum(s, c):
         cols = columns(c, chunk)
@@ -306,14 +322,12 @@
     def on_relay(task):
         pl.when(relaying == 1)(task)
 
-    def experts(g, amid=(), between=None, amid_down=()):
+    def extent(g):
         first, after = pass_starts[g], pass_starts[g + 1]
-        rows = block(first, after - first)
-        used = pl.ds(0, (after - first) * cap)
-        s = passes[g][1]
-        far = s is not None
-        own_far = len(passes[g][0]) * cap
-        has_own = 0 in passes[g][0]
+        return block(first, after - first), pl.ds(0, (after - first) * cap)
+
+    def gate_up(g, slot, amid=()):
+        rows, used = extent(g)
 
         @pl.loop(0, units // tile)
         def _(t):
@@ -327,21 +341,25 @@
             x = arrived[rows, :]
             gate = jnp.dot(x, gate_v[:, cols], preferred_element_type=jnp.float32)
             up = jnp.dot(x, up_v[:, cols], preferred_element_type=jnp.float32)
-            hidden[used, cols] = (gate / (1.0 + jnp.exp(-gate)) * up).astype(jnp.bfloat16)
-
-        if between is not None:
-            between()
+            hidden[slot, used, cols] = (gate / (1.0 + jnp.exp(-gate)) * up).astype(jnp.bfloat16)
+
+    def down(g, slot, turn, amid_down=()):
+        rows, used = extent(g)
+        s = passes[g][1]
+        far = s is not None
+        own_far = len(passes[g][0]) * cap
+        has_own = 0 in passes[g][0]
 
         @pl.loop(0, down_tiles)
         def _(t):
-            step = g * down_tiles + t
+            step = turn * down_tiles + t
             for when, role, task in amid_down:
                 here = (t == when) if role is None else (relaying == role) & (t == when)
                 pl.when(here)(task)
             load_down(step).wait()
             cols = columns(t, down_tile)
             result = jnp.dot(
-                hidden[used, :], down_v[step % depth], preferred_element_type=jnp.float32
+                hidden[slot, used, :], down_v[step % depth], preferred_element_type=jnp.float32
             ).astype(jnp.bfloat16)
             arrived[rows, cols] = result
             if has_own:
@@ -401,12 +419,9 @@
         pick(0, 0)
 
     on_relay(first_pick)
-    own_rows.wait()
     settle(near_part(arrived, 0, places), near_recv.at[0])
-    experts(
-        0, amid=[(8, 1, lambda: pick(0, 1))],
-        amid_down=[(0, 1, lambda: pick(0, 2))],
-    )
+    gate_up(0, 0, [(8, 1, lambda: pick(0, 1))])
+    down(0, 0, 0, [(0, 1, lambda: pick(0, 2))])
 
     def last_of_first():
         pick(0, chunks - 1)
@@ -434,34 +449,34 @@
         pick(1, 0)
 
     await_far(0)
-    experts(
-        1, amid=[(5, 1, first_of_second), (14, 1, lambda: pick(1, 1))],
-        amid_down=[(6, 1, lambda: pick(1, 2))],
-    )
+    gate_up(1, 0, [(5, 1, first_of_second), (14, 1, lambda: pick(1, 1))])
+    down(1, 0, 1, [(6, 1, lambda: pick(1, 2))])
+
     def last_of_second():
+        for c in range(2):
+            give_far(0, c, range(1, quarter))
         pick(1, chunks - 1)
-        for c in range(chunks):
+        for c in range(2, chunks):
             give_far(0, c, range(1, quarter))
 
     settle(near_part(arrived, 1, places), near_recv.at[1])
-    experts(
-        2, amid=[
-            (1, 1, last_of_second), (12, 1, lambda: relay_sum(0, 0)),
-            (15, 1, lambda: relay_sum(0, 1)),
-        ],
-        amid_down=[(4, 1, lambda: relay_sum(0, 2))],
-    )
-    on_relay(lambda: relay_sum(0, 3))
-
-    def relay_sums(s):
-        @pl.loop(0, chunks)
+    gate_up(2, 0, [(1, 1, last_of_second)])
+    down(2, 0, 2, [(2, 1, lambda: relay_sum(0, 0))])
+
+    def relay_sums(s, first):
+        @pl.loop(first, chunks)
         def _(c):
             relay_sum(s, c)
 
     await_far(1)
-    experts(3, amid=[(7, None, lambda: give_near(range(middle, half)))])
-    give_near(range(1, middle))
-    on_relay(lambda: relay_sums(1))
+    gate_up(
+        3, 0,
+        [(6 * c - 5, 1, functools.partial(relay_sum, 0, c)) for c in range(1, chunks)]
+        + [(9, None, lambda: give_near(range(middle, half)))],
+    )
+    down(3, 0, 3)
+    give_near(list(range(quarter, middle)) + list(range(1, quarter)))
+    on_relay(lambda: relay_sums(1, 0))
     for i in range(2):
         settle(near_part(near_back, i, plain), back_recv.at[i])
 
@@ -469,7 +484,7 @@
     def _(c):
         cols = columns(c, chunk)
         total[:, cols] = jnp.dot(
-            weights_v[...], near_back[:, cols], preferred_element_type=jnp.float32
+            near_weights[...], near_back[:, cols], preferred_element_type=jnp.float32
         )
 
     stream_in.wait()
@@ -479,7 +494,7 @@
 
     part = 32
 
-    @pl.loop(0, total.shape[0] // part)
+    @pl.loop(0, out_v.shape[0] // part)
     def _(t):
         some = pl.ds(pl.multiple_of(t * part, part), part)
         combined = total[some, :] + far_sum[some, :].astype(jnp.float32)
@@ -487,7 +502,7 @@
 
     settle(normed_hbm, tok_send.at[0])
     settle(meta_hbm, meta_send.at[0])
-    settle(rows_hbm.at[block(1, half - 1)], near_send.at[0])
+    settle(near_rows, near_send.at[0])
     for i in range(2):
         settle(near_part(arrived, i, places), back_send.at[i])
 
@@ -505,7 +520,7 @@
             settle(arrived.at[block(first_far[s], quarter)], far_send.at[s])
 
 
-def run_experts(outgoing, normed, meta, w_gate, w_up, w_down, weights, stream, gain, n, cap):
+def run_experts(normed, near_meta, meta, w_gate, w_up, w_down, stream, gain, n, cap):
     model_width, units = w_gate.shape[1], w_gate.shape[2]
     rows_blk = normed.shape[0]
     tile, down_tile, chunk, depth = 256, 256, model_width // 4, 4
@@ -528,14 +543,15 @@
     return pl.pallas_call(
         functools.partial(expert_kernel, n, cap, tile, down_tile, chunk),
         out_shape=jax.ShapeDtypeStruct(stream.shape, jnp.bfloat16),
-        in_specs=[anywhere] * 6 + [near] * 5 + [anywhere, near],
+        in_specs=[anywhere] * 5 + [near] * 5 + [anywhere, near],
         out_specs=near,
         scratch_shapes=[
             vmem((model_width, units), jnp.bfloat16),
             vmem((model_width, units), jnp.bfloat16),
             vmem((depth, units, down_tile), jnp.bfloat16),
             vmem((total_rows, model_width), jnp.bfloat16),
-            vmem((longest * cap, units), jnp.bfloat16),
+            vmem((1, longest * cap, units), jnp.bfloat16),
+            vmem(((half - 1) * cap, model_width), jnp.bfloat16),
             vmem((half * cap, model_width), jnp.bfloat16),
             vmem((rows_blk, model_width), jnp.bfloat16),
             vmem((2, rows_blk, model_width), jnp.bfloat16),
@@ -543,6 +559,7 @@
             vmem((2, half * cap, model_width), jnp.bfloat16),
             vmem((2,) + meta.shape, jnp.float32),
             vmem((half * cap, rows_blk), jnp.bfloat16),
+            vmem((rows_blk, half * cap), jnp.bfloat16),
             vmem((2, rows_blk, half * cap), jnp.bfloat16),
             vmem(stream.shape, jnp.float32),
             vmem(stream.shape, jnp.float32),
@@ -573,7 +590,7 @@
             bytes_accessed=6 * model_width * units,
             transcendentals=total_rows * units,
         ),
-    )(outgoing, normed, meta, w_gate, w_up, w_down, weights, *constants, stream, gain)
+    )(normed, meta, w_gate, w_up, w_down, near_meta, *constants, stream, gain)
 
 
 def per_device_whole(
@@ -622,26 +639,13 @@
     earlier_rows = jnp.asarray(np.tril(np.ones((rows_blk, rows_blk), np.float32), -1), jnp.bfloat16)
     rank = dot32(earlier_rows, hit.astype(jnp.bfloat16))
     place = jnp.where(hit, rank + 1.0, 0.0)
-    slots = np.arange(half * capacity)
-    spread = jnp.asarray(
-        (slots[None, :] // capacity == np.arange(half)[:, None]).astype(np.float32), jnp.bfloat16
-    )
-    wanted = jnp.asarray((slots % capacity + 1).astype(np.float32))
-    chosen = dot32(place[:, :half].astype(jnp.bfloat16), spread) == wanted[None, :]
-    outgoing = lax.dot_general(
-        chosen.astype(jnp.bfloat16),
-        normed,
-        (((0,), (0,)), ((), ())),
-        preferred_element_type=jnp.float32,
-    ).astype(jnp.bfloat16)
     shares = route_weights / jnp.sum(route_weights, axis=1, keepdims=True)
     share_of = jnp.sum(jnp.where(names, shares[:, :, None], 0.0), axis=1)
-    weights = jnp.where(
-        chosen, dot32(share_of[:, :half].astype(jnp.bfloat16), spread), 0.0
-    ).astype(jnp.bfloat16)
-    meta = jnp.concatenate([place[:, half:].T, share_of[:, half:].T], axis=0)
+    meta = jnp.concatenate([place.T, share_of.T], axis=0).reshape(2, 2, half, rows_blk)
+    near_meta = meta[:, 0].reshape(2 * half, rows_blk)
+    far_meta = meta[:, 1].reshape(2 * half, rows_blk)
     return run_experts(
-        outgoing, normed, meta, w_gate, w_up, w_down, weights, stream, norm_gains[2:3], experts, capacity
+        normed, near_meta, far_meta, w_gate, w_up, w_down, stream, norm_gains[2:3], experts, capacity
     )
 
 

time: 141 us -> 137 us (0.972)
  the two profiles are of different devices: /device:TPU:10 before, /device:TPU:9 now
where the time goes in v2:
time: 137 us
  Pallas kernels  116 us (85%)
  matrix products  6.64 us (5%)
  local copies, waits for them, and re-layouts  5.03 us (4%)
  other arithmetic  4.97 us (4%)
  starting transfers between devices  3.68 us (3%)
    pallas_call x1, Pallas kernels, run_experts(): pl.pallas_call(functools.partial(expert_kernel, n, cap, tile, down_tile,...  116 us
    dot_general x1, matrix products, per_device_whole(): jnp.dot(mixed_rows, out_weight, preferred_element_type=jnp.float32)  6.5 us
    ppermute x1, starting transfers between devices, passed_along(): return lax.ppermute(block, axis, route)  3.68 us
    unnamed x19, local copies, waits for them, and re-layouts  3.67 us
  transfers between devices with their start and end apart: 1, of which 0 were waited for; matrix products, arithmetic and copies ran while one was open for 1% of the time, Pallas kernels for 0%

profile of v2, /device:TPU:9, one launch (start us, length us, event | category | flops | bytes accessed | tf_op | source)
XLA Modules:
  0.0 136.7 jit_solution(2408632725892688219)
XLA Ops:
  0.0 0.7 convert_element_type.38
  0.7 0.1 slice.50
  0.8 0.0 copy-start.5
  0.8 0.0 copy-start.6
  0.8 0.0 copy-start.7
  0.8 0.0 copy-start.8
  0.8 2.0 %convert_multiply_fusion.2 = f32[256,2048]{1,0:T(8,128)S(1)} fusion(bf16[256,2048]{1,0:T(8,128)(2,1)} %param.21, bf16[256,2048]{1,0:T(8,128)(2,1)} %param.20), kind=kLoop, calls=%fused_computation.20 | loop fusion | flops 1572864 | bytes 4194304 | tf_op jit(solution)/shard_map/mul | solution.py:605
  2.9 3.7 %collective-permute-start = (f32[3,2048]{1,0:T(4,128)S(1)}, f32[3,2048]{1,0:T(4,128)S(1)}, u32[]{:S(2)}, u32[]{:S(2)}) collective-permute-start(f32[3,2048]{1,0:T(4,128)S(1)} %pad_maximum_fusion.1), channel_id=1, source_target_pairs={{0,1},{1,2},{2,3},{3,4},{4,5},{5,6},{6,7},{7,8},{8,9},{9,10},{10,1... | collective-permute-start | bytes 73736 | tf_op jit(solution)/shard_map/ppermute | solution.py:21
  6.6 0.0 copy-done.5
  6.6 0.1 pad_add_fusion
  6.7 0.0 copy-done.6
  6.7 0.1 compare_reduce_fusion
  6.8 0.1 fusion.20
  6.9 0.0 copy-done.3
  6.9 0.0 copy-done.4
  6.9 0.6 fusion.24
  7.5 0.0 copy-done.2
  7.5 0.1 fusion.12
  7.7 0.7 slice_bitcast_fusion
  8.3 0.0 collective-permute-done
  8.3 0.1 pad_maximum_fusion.3
  8.4 0.0 copy-done.7
  8.4 0.1 slice_compare_fusion.1
  8.5 0.0 copy-done.8
  8.5 0.0 copy-start.1
  8.5 6.5 %fusion.7 = (f32[256]{0:T(256)S(1)}, bf16[256,2048]{1,0:T(8,128)(2,1)S(1)}) fusion(bf16[2048,2048]{1,0:T(8,128)(2,1)} %param.24, f32[2,2048]{1,0:T(2,128)S(1)} %slice.68, f32[256,2048]{1,0:T(8,128)S(1)} %convert_multiply_fusion.2, bf16[256,2048]{1,0:T(8,128)(2,1)S(1)} %copy-done.8, f32[2048]{0:T(1024)S(1)} %bitcast.30, f32[2048]{0:T(1024)S(1)} %bitcast.29, ...), kind=kOutput, calls=%fused_computation.12 | convolution fusion | flops 2155872000 | bytes 12625408 | tf_op jit(solution)/shard_map/dot_general | solution.py:621
  15.0 0.0 copy-done.1
  15.0 0.6 multiply_reduce_fusion
  15.7 1.3 copy-done
  17.0 1.2 multiply_convert_fusion.normed_hbm
  18.2 116.2 %shard_map.172 = bf16[256,2048]{1,0:T(8,128)(2,1)} custom-call(bf16[256,2048]{1,0:T(8,128)(2,1)} %multiply_convert_fusion.normed_hbm, f32[16,256]{1,0:T(8,128)} %get-tuple-element.11.meta_hbm, bf16[1,2048,4096]{2,1,0:T(8,128)(2,1)} %gate_hbm.1, bf16[1,2048,4096]{2,1,0:T(8,128)(2,1)} %up_hbm.1, bf16[1,4096,2048]{2,1,0:T(8,128)(2,1)} %down_hbm.1, ...), custom_call_target="tpu_custom_call" | custom-call | flops 38654705664 | bytes 50331648 | tf_op jit(solution)/shard_map/pallas_call | solution.py:543
  134.4 2.3 %copy.28 = bf16[256,2048]{1,0:T(8,128)(2,1)} copy(bf16[256,2048]{1,0:T(8,128)(2,1)} %shard_map.172) | data formatting | bytes 2097152
  (16 shorter events, 0.1 us)
Async XLA Ops:
  0.8 5.9 %copy-start.5 = (f32[256,2]{0,1:T(2,128)S(1)}, f32[256,2]{0,1:T(2,128)}, u32[]{:S(2)}) copy-start(f32[256,2]{0,1:T(2,128)} %param.27) | copy-start | bytes 6148
  0.8 6.0 %copy-start.6 = (s32[256,2]{0,1:T(2,128)S(1)}, s32[256,2]{0,1:T(2,128)}, u32[]{:S(2)}) copy-start(s32[256,2]{0,1:T(2,128)} %param.26) | copy-start | bytes 6148
  0.8 6.1 %copy-start.3 = (bf16[3,2048]{1,0:T(4,128)(2,1)S(1)}, bf16[3,2048]{1,0:T(4,128)(2,1)}, u32[]{:S(2)}) copy-start(bf16[3,2048]{1,0:T(4,128)(2,1)} %param.22) | copy-start | bytes 36868
  0.8 6.1 %copy-start.4 = (f32[3,2048]{1,0:T(4,128)S(1)}, f32[3,2048]{1,0:T(4,128)}, u32[]{:S(2)}) copy-start(f32[3,2048]{1,0:T(4,128)} %param.25) | copy-start | bytes 73732
  0.8 6.7 %copy-start.2 = (bf16[256,256]{1,0:T(8,128)(2,1)S(1)}, bf16[256,256]{1,0:T(8,128)(2,1)}, u32[]{:S(2)}) copy-start(bf16[256,256]{1,0:T(8,128)(2,1)} %constant.63.clone) | copy-start | bytes 393220
  0.8 7.6 %copy-start.7 = (s32[256]{0:T(256)S(1)}, s32[256]{0:T(256)}, u32[]{:S(2)}) copy-start(s32[256]{0:T(256)} %param.23) | copy-start | bytes 3076
  0.8 7.7 %copy-start.8 = (bf16[256,2048]{1,0:T(8,128)(2,1)S(1)}, bf16[256,2048]{1,0:T(8,128)(2,1)}, u32[]{:S(2)}) copy-start(bf16[256,2048]{1,0:T(8,128)(2,1)} %param.19) | copy-start | bytes 3145732
  2.9 5.5 %collective-permute-start = (f32[3,2048]{1,0:T(4,128)S(1)}, f32[3,2048]{1,0:T(4,128)S(1)}, u32[]{:S(2)}, u32[]{:S(2)}) collective-permute-start(f32[3,2048]{1,0:T(4,128)S(1)} %pad_maximum_fusion.1), channel_id=1, source_target_pairs={{0,1},{1,2},{2,3},{3,4},{4,5},{5,6},{6,7},{7,8},{8,9},{9,10},{10,1... | collective-permute-start | bytes 73736 | tf_op jit(solution)/shard_map/ppermute | solution.py:21
  8.5 6.5 %copy-start.1 = (bf16[256,2048]{1,0:T(8,128)(2,1)S(1)}, bf16[256,2048]{1,0:T(8,128)(2,1)}, u32[]{:S(2)}) copy-start(bf16[256,2048]{1,0:T(8,128)(2,1)} %param.18) | copy-start | bytes 3145732
  15.7 1.3 copy-start
